TPU v7x, 256 devices: a whole 4x4x8 slice. The times are simulated.
256 devices in a mesh: ep: 16 (over y, x), tp: 16 (over z, core).
Axes of the slice: x: 4, y: 4, z: 8, core: 2. Of those that a mesh axis runs over, the one named last changes fastest.
Arguments:
- pool_input: bfloat16 [32768, 1024], P('ep', 'tp'), may hold values from -6 to 6
- pool_gain: float32 [1024], P('tp'), may hold values from 0.1 to 1.9
- mix_weight: bfloat16 [1024, 2048], P('tp'), may hold values from -0.1875 to 0.1875
- moe_input: bfloat16 [65536, 2048], P(('ep', 'tp')), may hold values from -6 to 6
- moe_gain: float32 [2048], replicated, may hold values from 0.1 to 1.9
- expert_ids: int32 [65536, 2], P(('ep', 'tp')), may hold values from 0 to 15, as said below
- route_weight: float32 [65536, 2], P(('ep', 'tp')), may hold values from 0.2 to 1
- gate_weight: bfloat16 [16, 2048, 1024], P('ep', None, 'tp'), may hold values from -0.125 to 0.125
- up_weight: bfloat16 [16, 2048, 1024], P('ep', None, 'tp'), may hold values from -0.125 to 0.125
- down_weight: bfloat16 [16, 2048, 1024], P('ep', None, 'tp'), may hold values from -0.1875 to 0.1875
Outputs:
- mixed_out: bfloat16 [32768, 2048], P(('ep', 'tp'))
- moe_out: bfloat16 [65536, 2048], P(('ep', 'tp'))
Inputs may be any that keep to these rules, and one draw needn't show every extreme that they name: `expert_ids`: each row names 2 different experts of one group of 4 consecutive experts. In each aligned block of 256 rows (the rows of one device) no expert is named by more than 48 rows, and some expert is named by exactly 48 rows.
All inputs are finite; a program needn't handle non-finite values.
Results may differ from a plain program's by a relative error of at most 0.012.
Values may be sent and summed in bfloat16 or wider, within the bound.
A program may use at most 128 MiB of HBM per device.

v0:
```python
import jax
import jax.numpy as jnp
from jax import lax
from jax.sharding import PartitionSpec as P

GROUP_CH = 256
EXPERTS = 16
TOP = 2
CAP = 48


eps_norm = 1e-06


def from_behind(shard, axis, by):
    peers = lax.axis_size(axis)
    pairs = [(i, i + by) for i in range(peers) if 0 <= i + by < peers]
    return lax.ppermute(shard, axis, pairs)


def gather_turned(arrays, axis, dims):
    turned = [jnp.moveaxis(a, dim, 0) for a, dim in zip(arrays, dims)]
    both = jnp.concatenate([t.reshape(len(t), -1) for t in turned], axis=1)
    result, at, gathered = (lax.all_gather(both, axis, axis=0, tiled=True), 0, [])
    for t, dim in zip(turned, dims):
        section = result[:, at : at + t[0].size].reshape(-1, *t.shape[1:])
        gathered.append(jnp.moveaxis(section, 0, dim))
        at += t[0].size
    return tuple(gathered)


def in_blocks(shard, dim, peers):
    before, after = (shard.shape[:dim], shard.shape[dim + 1 :])
    return jnp.moveaxis(shard.reshape(*before, peers, -1, *after), dim, 0)


def cut_rows(length, count):
    unit = 8 if length >= 8 * count else 1
    return [length // unit * k // count * unit for k in range(1, count)]


def joined_along(tiles, dim):
    tiles = jnp.moveaxis(tiles, 0, dim)
    dims = tiles.shape
    return tiles.reshape(*dims[:dim], dims[dim] * dims[dim + 1], *dims[dim + 2 :])


def exchange_in_pieces(shard, axis, pieces, split_dim, concat_dim):
    tiles = in_blocks(shard, split_dim, lax.axis_size(axis))
    widest = max(range(1, max(2, tiles.ndim - 1)), key=lambda d: tiles.shape[d])
    gathered = []
    for section in jnp.split(tiles, cut_rows(tiles.shape[widest], pieces), axis=widest):
        if section.size:
            gathered.append(lax.all_to_all(section, axis, split_axis=0, concat_axis=0, tiled=True))
    return joined_along(jnp.concatenate(gathered, axis=widest), concat_dim)


def window_sums(extended, row_count):
    level_sum = extended
    stride = 1
    outputs = []
    for doubling in range(4):
        level_sum = level_sum[stride:] + level_sum[:-stride]
        stride = stride * 2
        outputs.append(level_sum[level_sum.shape[0] - row_count :])
    return outputs


def pool_mixer(pool_input, pool_gain):
    row_count, channels = pool_input.shape
    carried = from_behind(pool_input[row_count - 15 :], "ep", 1)
    extended = jnp.concatenate([carried, pool_input], axis=0).astype(jnp.float32)
    window_list = window_sums(extended, row_count)
    channel_ids = lax.axis_index("tp") * channels + lax.iota(jnp.int32, channels)
    group_ids = channel_ids // GROUP_CH
    position = lax.axis_index("ep") * row_count + lax.iota(jnp.int32, row_count)
    summed = jnp.zeros((row_count, channels), jnp.float32)
    widths = jnp.zeros((channels,), jnp.int32)
    for index_group in range(4):
        inside = group_ids == index_group
        summed = jnp.where(inside[None, :], window_list[index_group], summed)
        widths = jnp.where(inside, 2 ** (index_group + 1), widths)
    counted = jnp.minimum(position[:, None] + 1, widths[None, :]).astype(jnp.float32)
    values = extended[15:]
    return ((summed / counted - values) * pool_gain).astype(jnp.bfloat16)


def route_slots(expert_ids):
    flat_ids = expert_ids.reshape(-1)
    marked = (flat_ids[:, None] == lax.iota(jnp.int32, EXPERTS)[None, :]).astype(jnp.int32)
    before_count = jnp.cumsum(marked, axis=0) - marked
    ranked = jnp.sum(before_count * marked, axis=1)
    return (flat_ids * CAP + ranked).reshape(expert_ids.shape)


def body(
    pool_input,
    pool_gain,
    mix_weight,
    moe_input,
    moe_gain,
    expert_ids,
    route_weight,
    gate_weight,
    up_weight,
    down_weight,
):
    pooled = pool_mixer(pool_input, pool_gain)
    mixed_sum = lax.psum_scatter(
        jnp.dot(pooled, mix_weight, preferred_element_type=jnp.float32).astype(jnp.bfloat16),
        "tp",
        scatter_dimension=0,
        tiled=True,
    )
    inputs = moe_input.astype(jnp.float32)
    scale_rows = lax.rsqrt(jnp.mean(inputs * inputs, axis=-1, keepdims=True) + eps_norm)
    normed = (inputs * scale_rows * moe_gain).astype(jnp.bfloat16)
    slots = route_slots(expert_ids)
    slot_index = lax.iota(jnp.int32, EXPERTS * CAP)
    placing = (
        (slot_index[:, None] == slots[None, :, 0]) | (slot_index[:, None] == slots[None, :, 1])
    ).astype(jnp.bfloat16)
    outgoing = jnp.dot(placing, normed, preferred_element_type=jnp.float32).astype(jnp.bfloat16)
    outgoing = outgoing.reshape(EXPERTS, CAP, normed.shape[1])
    arrived = lax.all_to_all(outgoing, "ep", split_axis=0, concat_axis=1, tiled=True)
    gate_piece, up_piece, down_piece = gather_turned(
        (gate_weight, up_weight, down_weight), "tp", (2, 2, 2)
    )
    gate_part = jnp.einsum("erd,edf->erf", arrived, gate_piece, preferred_element_type=jnp.float32)
    upward = jnp.einsum("erd,edf->erf", arrived, up_piece, preferred_element_type=jnp.float32)
    hidden = (jax.nn.silu(gate_part) * upward).astype(jnp.bfloat16)
    expert_sum = jnp.einsum("erf,edf->erd", hidden, down_piece, preferred_element_type=jnp.float32)
    expert_rows = expert_sum.astype(jnp.bfloat16)
    returned = exchange_in_pieces(expert_rows, "ep", 2, 1, 0)
    returned_rows = returned.reshape(EXPERTS * CAP, returned.shape[2])
    combined = jnp.zeros((normed.shape[0], normed.shape[1]), jnp.float32)
    for route_index in range(TOP):
        picking = (slots[:, route_index][:, None] == slot_index[None, :]).astype(jnp.bfloat16)
        chosen_rows = jnp.dot(picking, returned_rows, preferred_element_type=jnp.float32)
        combined = combined + route_weight[:, route_index : route_index + 1] * chosen_rows
    moe_out = combined.astype(jnp.bfloat16)
    return (mixed_sum, moe_out)


def solution(mesh):
    return jax.shard_map(
        body,
        mesh=mesh,
        in_specs=(
            P("ep", "tp"),
            P("tp"),
            P("tp", None),
            P(("ep", "tp"), None),
            P(),
            P(("ep", "tp"), None),
            P(("ep", "tp"), None),
            P("ep", None, "tp"),
            P("ep", None, "tp"),
            P("ep", None, "tp"),
        ),
        out_specs=(P(("ep", "tp"), None), P(("ep", "tp"), None)),
        check_vma=False,
    )
```

profile of v0, /device:TPU:1, one launch (start us, length us, event | category | flops | bytes accessed | tf_op | source)
XLA Modules:
  0.0 168.6 jit_solution(2128738845076339087)
XLA Ops:
  7.2 0.0 copy-start
  7.2 0.0 all-gather.2.cloned.1.call-start
  7.2 2.1 %pad_maximum_fusion.1 = bf16[64,6144]{1,0:T(8,128)(2,1)} fusion(bf16[64,2048]{1,0:T(8,128)(2,1)} %bitcast.76, bf16[64,2048]{1,0:T(8,128)(2,1)} %bitcast.77, bf16[64,2048]{1,0:T(8,128)(2,1)} %bitcast.78), kind=kLoop, calls=%fused_computation.22 | loop fusion | flops 2359296 | bytes 1572864 | tf_op jit(solution)/shard_map/concatenate | solution.py:23
  9.3 0.0 all-gather.2.cloned.1.call-update
  9.3 0.0 copy-start.4
  9.3 0.0 reduce-scatter.2.cloned.1.call-start
  9.4 0.8 slice.66
  10.2 3.9 %collective-permute-start = (bf16[15,64]{0,1:T(8,128)(2,1)S(1)}, bf16[15,64]{0,1:T(8,128)(2,1)S(1)}, u32[]{:S(2)}, u32[]{:S(2)}) collective-permute-start(bf16[15,64]{0,1:T(8,128)(2,1)S(1)} %slice.66), channel_id=1, source_target_pairs={{0,16},{16,32},{32,48},{48,64},{64,80},{80,96},{96,112},{112,128},... | collective-permute-start | bytes 5768 | tf_op jit(solution)/shard_map/ppermute | solution.py:18
  14.2 0.8 collective-permute-done
  15.0 1.1 maximum_convert_fusion
  16.1 0.2 slice_add_fusion.2
  16.3 0.2 slice_add_fusion.1
  16.5 0.2 slice_add_fusion
  16.7 0.0 copy-done
  16.7 0.0 copy-done.4
  16.7 6.4 %convolution_convert_fusion = bf16[2048,2048]{1,0:T(8,128)(2,1)} fusion(bf16[64,2048]{1,0:T(8,128)(2,1)S(1)} %copy-done, f32[2063,64]{0,1:T(8,128)S(1)} %maximum_convert_fusion, f32[2062,64]{0,1:T(8,128)S(1)} %slice_add_fusion.2, f32[2060,64]{0,1:T(8,128)S(1)} %slice_add_fusion.1, f32[2056,64]{0,1:T(8,128)S(1)} %slice_add_fusion, f32[64]{0:T(128)S(1)} %copy-done.4, ...), kind=kOutput, calls=%fused_computation | convolution fusion | flops 542507008 | bytes 11283456 | tf_op jit(solution)/shard_map/dot_general | solution.py:110
  23.1 0.0 copy-start.3
  23.1 0.0 copy-start.1
  23.1 0.0 copy-start.2
  23.1 0.0 reduce-scatter.2.cloned.1.call-update
  23.2 0.7 copy-done.3
  23.8 0.1 copy.29
  23.9 0.1 eq.138
  24.1 0.1 eq.134
  24.3 1.2 reduce-window.6
  25.4 0.2 slice_reduce_fusion
  25.7 0.1 fusion.35
  25.8 0.1 reduce_sum.21
  25.9 0.1 copy.32
  26.0 0.0 copy-done.1
  26.0 0.3 fusion.6
  26.3 0.0 copy-done.2
  26.3 1.1 convolution_convert_fusion.1
  27.5 45.8 %all_to_all.19 = bf16[16,48,2048]{2,1,0:T(8,128)(2,1)S(1)} all-to-all(bf16[16,48,2048]{2,1,0:T(8,128)(2,1)S(1)} %bitcast.72), channel_id=1, replica_groups=mesh['ep'=16,'tp'=16] {'ep'}, dimensions={0} | all-to-all | bytes 6291456 | tf_op jit(solution)/shard_map/all_to_all | solution.py:125
  73.3 16.9 %all-gather.2.cloned.1.call-done = bf16[1024,6144]{1,0:T(8,128)(2,1)} async-done(((bf16[64,6144]{1,0:T(8,128)(2,1)}), bf16[1024,6144]{1,0:T(8,128)(2,1)}) %all-gather.2.cloned.1.call-update) | async-done | bytes 12582928 | tf_op jit(solution)/shard_map/all_gather | solution.py:24
  90.2 0.0 copy-start.6
  90.2 5.4 %fusion.1 = f32[768,1024]{1,0:T(8,128)S(1)} fusion(bf16[768,2048]{1,0:T(8,128)(2,1)S(1)} %bitcast.73, bf16[1024,6144]{1,0:T(8,128)(2,1)} %all-gather.2.cloned.1.call-done), kind=kOutput, calls=%fused_computation.4 | convolution fusion | flops 3221225472 | bytes 10485760 | tf_op jit(solution)/shard_map/erd,edf->erf/dot_general | solution.py:130
  95.7 0.4 copy-done.6
  96.1 3.9 %multiply_convert_fusion = bf16[768,1024]{1,0:T(8,128)(2,1)S(1)} fusion(f32[768,1024]{1,0:T(8,128)S(1)} %fusion.1, bf16[768,2048]{1,0:T(8,128)(2,1)S(1)} %bitcast.74, bf16[1024,6144]{1,0:T(8,128)(2,1)S(1)} %copy-done.6), kind=kOutput, calls=%fused_computation.10 | convolution fusion | flops 3225944064 | bytes 12058624 | tf_op jit(solution)/shard_map/erd,edf->erf/dot_general | solution.py:129
  99.9 3.6 %fusion.3 = bf16[768,2048]{1,0:T(8,128)(2,1)S(1)} fusion(bf16[768,1024]{1,0:T(8,128)(2,1)S(1)} %multiply_convert_fusion, bf16[1024,6144]{1,0:T(8,128)(2,1)S(1)} %copy-done.6), kind=kOutput, calls=%fused_computation.7 | convolution fusion | flops 3222798336 | bytes 8912896 | tf_op jit(solution)/shard_map/erf,edf->erd/dot_general | solution.py:132
  103.6 1.4 fusion.38
  105.0 0.0 copy-start.5
  105.0 28.5 %all_to_all.20 = bf16[16,1,24,2048]{3,2,1,0:T(8,128)(2,1)S(1)} all-to-all(bf16[16,1,24,2048]{3,2,1,0:T(8,128)(2,1)S(1)} %get-tuple-element.2), channel_id=1, replica_groups=mesh['ep'=16,'tp'=16] {'ep'}, dimensions={0} | all-to-all | bytes 3145728 | tf_op jit(solution)/shard_map/all_to_all | solution.py:54
  133.5 3.7 %all-to-all-start.2 = ((bf16[16,1,24,2048]{3,2,1,0:T(8,128)(2,1)}), bf16[16,1,24,2048]{3,2,1,0:T(8,128)(2,1)S(1)}, u32[]{:S(2)}, u32[]{:S(2)}) async-start(bf16[16,1,24,2048]{3,2,1,0:T(8,128)(2,1)} %get-tuple-element.3), calls=%async_computation.3 | async-start | bytes 3145728 | tf_op jit(solution)/shard_map/all_to_all | solution.py:54
  137.2 0.0 copy-done.5
  137.2 20.9 %all-to-all-done.2 = bf16[16,1,24,2048]{3,2,1,0:T(8,128)(2,1)S(1)} async-done(((bf16[16,1,24,2048]{3,2,1,0:T(8,128)(2,1)}), bf16[16,1,24,2048]{3,2,1,0:T(8,128)(2,1)S(1)}, u32[]{:S(2)}, u32[]{:S(2)}) %all-to-all-start.2) | async-done | bytes 1572896 | tf_op jit(solution)/shard_map/all_to_all | solution.py:54
  158.1 0.4 pad_maximum_fusion
  158.5 1.1 convolution_multiply_fusion.1
  159.6 2.1 %fusion.5 = bf16[256,2048]{1,0:T(8,128)(2,1)} fusion(f32[256,2048]{1,0:T(8,128)S(1)} %convolution_multiply_fusion.1, bf16[768,2048]{1,0:T(8,128)(2,1)S(1)} %bitcast.71, f32[256]{0:T(256)S(1)} %bitcast.81, s32[256]{0:T(256)S(1)} %bitcast.80), kind=kOutput, calls=%fused_computation.16 | convolution fusion | flops 807075840 | bytes 6293504 | tf_op jit(solution)/shard_map/dot_general | solution.py:139
  161.7 0.0 reduce-scatter.2.cloned.1.call-done
  (11 shorter events, 0.1 us)
Async XLA Ops:
  7.2 9.6 %copy-start = (bf16[64,2048]{1,0:T(8,128)(2,1)S(1)}, bf16[64,2048]{1,0:T(8,128)(2,1)}, u32[]{:S(2)}) copy-start(bf16[64,2048]{1,0:T(8,128)(2,1)} %param.12) | copy-start | bytes 786436
  7.2 83.0 %all-gather.2.cloned.1.call-start = ((), (), s32[]{:S(2)}) async-start(), calls=%async_computation.5 | async-start | bytes 13369344 | tf_op jit(solution)/shard_map/all_gather | solution.py:24
  9.3 7.4 %copy-start.4 = (f32[64]{0:T(128)S(1)}, f32[64]{0:T(128)}, u32[]{:S(2)}) copy-start(f32[64]{0:T(128)} %param.11) | copy-start | bytes 772
  9.3 152.4 %reduce-scatter.2.cloned.1.call-start = ((), (), s32[]{:S(2)}) async-start(), calls=%async_computation.4 | async-start | bytes 8912896 | tf_op jit(solution)/shard_map/reduce_scatter | solution.py:109
  10.2 4.8 %collective-permute-start = (bf16[15,64]{0,1:T(8,128)(2,1)S(1)}, bf16[15,64]{0,1:T(8,128)(2,1)S(1)}, u32[]{:S(2)}, u32[]{:S(2)}) collective-permute-start(bf16[15,64]{0,1:T(8,128)(2,1)S(1)} %slice.66), channel_id=1, source_target_pairs={{0,16},{16,32},{32,48},{48,64},{64,80},{80,96},{96,112},{112,128},... | collective-permute-start | bytes 5768 | tf_op jit(solution)/shard_map/ppermute | solution.py:18
  23.1 0.7 copy-start.3
  23.1 2.9 %copy-start.1 = (bf16[256,2048]{1,0:T(8,128)(2,1)S(1)}, bf16[256,2048]{1,0:T(8,128)(2,1)}, u32[]{:S(2)}) copy-start(bf16[256,2048]{1,0:T(8,128)(2,1)} %param.13) | copy-start | bytes 3145732
  23.1 3.2 %copy-start.2 = (f32[2048]{0:T(1024)S(1)}, f32[2048]{0:T(1024)}, u32[]{:S(2)}) copy-start(f32[2048]{0:T(1024)} %param.14) | copy-start | bytes 24580
  90.2 5.8 %copy-start.6 = (bf16[1024,6144]{1,0:T(8,128)(2,1)S(1)}, bf16[1024,6144]{1,0:T(8,128)(2,1)}, u32[]{:S(2)}) copy-start(bf16[1024,6144]{1,0:T(8,128)(2,1)} %all-gather.2.cloned.1.call-done) | copy-start | bytes 37748740
  105.0 32.2 %copy-start.5 = (f32[256,2]{0,1:T(2,128)S(1)}, f32[256,2]{0,1:T(2,128)}, u32[]{:S(2)}) copy-start(f32[256,2]{0,1:T(2,128)} %param.16) | copy-start | bytes 6148
  133.5 24.7 %all-to-all-start.2 = ((bf16[16,1,24,2048]{3,2,1,0:T(8,128)(2,1)}), bf16[16,1,24,2048]{3,2,1,0:T(8,128)(2,1)S(1)}, u32[]{:S(2)}, u32[]{:S(2)}) async-start(bf16[16,1,24,2048]{3,2,1,0:T(8,128)(2,1)} %get-tuple-element.3), calls=%async_computation.3 | async-start | bytes 3145728 | tf_op jit(solution)/shard_map/all_to_all | solution.py:54
Sparse Core Ops, SparseCore 0:
  10.4 79.7 all-gather.1
  93.3 66.8 reduce-scatter.1
where the time goes:
time: 170 us; the launch traced here: 169 us
  blocking collectives  74.3 us (44%)
  waiting for transfers between devices  38.6 us (23%)
  matrix products  23.6 us (14%)
  between operations  14.3 us (8%)
  starting transfers between devices  7.71 us (5%)
  other arithmetic  5.79 us (3%)
  local copies, waits for them, and re-layouts  4.17 us (2%)
    all_to_all x1, blocking collectives, body(): lax.all_to_all(outgoing, 'ep', split_axis=0, concat_axis=1, tiled=True)  45.8 us
    all_to_all x1, blocking collectives, exchange_in_pieces(): lax.all_to_all(section, axis, split_axis=0, concat_axis=0, tiled=True)  28.5 us
    all_to_all x1, waiting for transfers between devices, exchange_in_pieces(): lax.all_to_all(section, axis, split_axis=0, concat_axis=0, tiled=True)  20.9 us
    all_gather x1, waiting for transfers between devices, gather_turned(): lax.all_gather(both, axis, axis=0, tiled=True)  16.9 us
    dot_general x1, matrix products, body(): jnp.dot(pooled, mix_weight, preferred_element_type=jnp.float32)  6.39 us
    dot_general x1, matrix products, body(): jnp.einsum('erd,edf->erf', arrived, up_piece, preferred_element_type=jnp....  5.42 us
    ppermute x1, starting transfers between devices, from_behind(): return lax.ppermute(shard, axis, pairs)  3.92 us
    dot_general x1, matrix products, body(): jnp.einsum('erd,edf->erf', arrived, gate_piece, preferred_element_type=jn...  3.85 us
  transfers between devices with their start and end apart: 4, of which 3 were waited for; matrix products, arithmetic and copies ran while one was open for 18% of the time, Pallas kernels for 0%

commit v1 on v0

v1 whole, which is shorter than its diff:
```python
import functools

import jax
import jax.numpy as jnp
from jax import lax
from jax.experimental import pallas as pl
from jax.experimental.pallas import tpu as pltpu
from jax.sharding import PartitionSpec as P

GROUP_CH = 256
EXPERTS = 16
CAP = 48
NX, NY, NZ = 4, 4, 8
EPS_NORM = 1e-06
DEV = pl.DeviceIdType.MESH

OFFSETS = (
    (0, 0), (1, 1), (3, 3), (0, 1), (0, 3), (2, 2), (1, 3), (3, 1),
    (1, 0), (3, 0), (2, 1), (2, 3), (1, 2), (3, 2), (0, 2), (2, 0),
)
SLOT_OF = {0: 0, 1: 1, -1: 2, 2: 3, -2: 4, 3: 5, -3: 6, 4: 7, -4: 7}
CW, CCW = 0, 1


def wait_for(ref, sem):
    pltpu.make_async_copy(ref, ref, sem).wait()


def kernel(
    gate_hbm, up_hbm, down_hbm, mix_hbm, pool_hbm, x_hbm,
    pool_gain, moe_gain, ids_ref, route_ref,
    mixed_hbm, moe_hbm,
    w_gate, w_up, w_down, w_mix,
    pool_in, halo, pooled, pooled_all, x_in, normed, placing, picking,
    outgoing, arrived, hidden, rows_out, rows_back, moe_vmem, mixed_vmem,
    load_sem, store_sem, ring_recv, ring_send, push_send, sib_gate, sib_up, sib_down, sib_mix,
    disp_send, disp_recv, halo_sem, pool_sem, ret_send, ret_recv,
):
    ep = lax.axis_index("ep")
    tp = lax.axis_index("tp")
    px, py = lax.rem(ep, NX), ep // NX
    pz, core = tp // 2, lax.rem(tp, 2)

    def plane(dx, dy):
        return (lax.rem(py + dy, NY) * NX + lax.rem(px + dx, NX), tp)

    def column(dz, dc):
        return (ep, lax.rem(pz + dz, NZ) * 2 + lax.rem(core + dc, 2))

    sibling = column(0, 1)
    ring_to = {CW: column(1, 0), CCW: column(NZ - 1, 0)}

    barrier = pltpu.get_barrier_semaphore()
    for dx, dy in OFFSETS[1:]:
        pl.semaphore_signal(barrier, inc=1, device_id=plane(dx, dy), device_id_type=DEV)
    for dz in range(NZ):
        for dc in range(2):
            if (dz, dc) != (0, 0):
                pl.semaphore_signal(barrier, inc=1, device_id=column(dz, dc), device_id_type=DEV)

    def piece(ref, index=None):
        def at(slot, other):
            rows = pl.ds(slot * 128 + 64 * other, 64)
            return ref.at[rows] if index is None else ref.at[index, rows]

        return at

    pieces = {"g": piece(w_gate), "u": piece(w_up)}
    hops = {"g": (4, 3), "u": (3, 4)}
    span = {"g": w_gate, "u": w_up}
    for q in range(4):
        pieces[f"d{q}"] = piece(w_down, q)
        hops[f"d{q}"] = (4, 3) if q % 2 == 0 else (3, 4)
        span[f"d{q}"] = w_down.at[q]
    for h in range(2):
        pieces[f"m{h}"] = piece(w_mix, h)
        hops[f"m{h}"] = (4, 3) if h == 0 else (3, 4)
        span[f"m{h}"] = w_mix.at[h]
    names = list(pieces)
    number = {name: k for k, name in enumerate(names)}

    loads = {}

    def load(name, src, dst):
        copy = pltpu.make_async_copy(src, dst, load_sem.at[len(loads)])
        copy.start()
        loads[name] = copy

    load("g", gate_hbm, w_gate.at[pl.ds(0, 64)])
    load("u", up_hbm, w_up.at[pl.ds(0, 64)])
    load("d0", down_hbm.at[:, pl.ds(0, 512)], w_down.at[0, pl.ds(0, 64)])
    load("x", x_hbm, x_in)
    load("pool", pool_hbm, pool_in)
    for q in range(1, 4):
        load(f"d{q}", down_hbm.at[:, pl.ds(512 * q, 512)], w_down.at[q, pl.ds(0, 64)])
    for h in range(2):
        load(f"m{h}", mix_hbm.at[:, pl.ds(1024 * h, 1024)], w_mix.at[h, pl.ds(0, 64)])

    def sib_sem(name, slot):
        if name == "g":
            return sib_gate.at[(0, 0, 0, 0, 1, 1, 2, 2)[slot]]
        if name == "u":
            return sib_up.at[(0, 0, 0, 0, 1, 1, 2, 2)[slot]]
        if name[0] == "d":
            return sib_down.at[int(name[1])]
        return sib_mix.at[int(name[1])]

    def ring_copy(name, way, hop):
        sign = -1 if way == CW else 1
        source, target = SLOT_OF[sign * (hop - 1)], SLOT_OF[sign * hop]
        at = pieces[name]
        return pltpu.make_async_remote_copy(
            src_ref=at(source, 0),
            dst_ref=at(target, 0),
            send_sem=ring_send.at[number[name]],
            recv_sem=ring_recv.at[number[name], way * 4 + hop - 1],
            device_id=ring_to[way],
            device_id_type=DEV,
        )

    def push(name, slot):
        at = pieces[name]
        pltpu.make_async_remote_copy(
            src_ref=at(slot, 0),
            dst_ref=at(slot, 1),
            send_sem=push_send.at[number[name]],
            recv_sem=sib_sem(name, slot),
            device_id=sibling,
            device_id_type=DEV,
        ).start()

    def first_sends(*pairs):
        for name, way in pairs:
            ring_copy(name, way, 1).start()

    def arrival(name, way, hop):
        if hop > hops[name][way]:
            return
        ring_copy(name, way, hop).wait_recv()
        if hop < hops[name][way]:
            ring_copy(name, way, hop + 1).start()
        push(name, SLOT_OF[-hop if way == CW else hop])

    def arrivals(hop, *pairs):
        for name, way in pairs:
            arrival(name, way, hop)

    set_one = (("g", CW), ("u", CCW), ("u", CW), ("g", CCW), ("d0", CW), ("d0", CCW))
    set_two = tuple((f"d{q}", way) for q in (1, 2, 3) for way in (CCW, CW))
    set_mix = (("m0", CW), ("m1", CCW), ("m1", CW), ("m0", CCW))

    pl.semaphore_wait(barrier, 30)

    loads["g"].wait()
    first_sends(("g", CW))
    loads["u"].wait()
    first_sends(*set_one[1:4])
    loads["d0"].wait()
    first_sends(*set_one[4:])

    loads["pool"].wait()
    halo_copy = pltpu.make_async_remote_copy(
        src_ref=pool_in.at[:, pl.ds(pool_in.shape[1] - 128, 128)],
        dst_ref=halo,
        send_sem=halo_sem.at[0],
        recv_sem=halo_sem.at[1],
        device_id=(lax.rem(ep + 1, EXPERTS), tp),
        device_id_type=DEV,
    )
    halo_copy.start()

    for name in ("g", "u", "d0"):
        push(name, 0)

    loads["x"].wait()
    gain_row = moe_gain[...]

    def norm_rows(k, carry):
        rows = pl.ds(k * 64, 64)
        v = x_in[rows, :].astype(jnp.float32)
        scale = lax.rsqrt(jnp.mean(v * v, axis=-1, keepdims=True) + EPS_NORM)
        normed[rows, :] = (v * scale * gain_row).astype(jnp.bfloat16)
        return carry

    lax.fori_loop(0, 4, norm_rows, 0)

    tokens = x_in.shape[0]
    expert = lax.broadcasted_iota(jnp.int32, (EXPERTS, tokens), 0)
    ids = ids_ref[...]
    chosen = [(ids[k : k + 1, :] == expert).astype(jnp.float32) for k in range(2)]
    marked = (chosen[0] + chosen[1]).astype(jnp.bfloat16)
    before = (
        lax.broadcasted_iota(jnp.int32, (tokens, tokens), 0)
        < lax.broadcasted_iota(jnp.int32, (tokens, tokens), 1)
    ).astype(jnp.bfloat16)
    rank = jnp.dot(marked, before, preferred_element_type=jnp.float32)
    away = lax.rem(expert // NX - py + NY, NY) * NX + lax.rem(lax.rem(expert, NX) - px + NX, NX)
    place = jnp.zeros((EXPERTS, tokens), jnp.float32)
    for p, (dx, dy) in enumerate(OFFSETS):
        place = jnp.where(away == dy * NX + dx, float(p * CAP), place)
    slot_of = place + rank
    slots = [
        jnp.sum(chosen[k] * slot_of, axis=0, keepdims=True).astype(jnp.int32) for k in range(2)
    ]

    def disp_copy(p):
        dx, dy = OFFSETS[p]
        rows = pl.ds(p * CAP, CAP)
        return pltpu.make_async_remote_copy(
            src_ref=outgoing.at[rows],
            dst_ref=arrived.at[rows],
            send_sem=disp_send,
            recv_sem=disp_recv.at[0 if p < 8 else 1],
            device_id=plane(dx, dy),
            device_id_type=DEV,
        )

    for group in range(4):
        row_ids = lax.broadcasted_iota(jnp.int32, (4 * CAP, tokens), 0) + group * 4 * CAP
        hit = (row_ids == slots[0]) | (row_ids == slots[1])
        placing[...] = hit.astype(jnp.bfloat16)

        def place_columns(n, carry, group=group):
            cols = pl.ds(pl.multiple_of(n * 512, 512), 512)
            block = jnp.dot(
                placing[...], normed[:, cols], preferred_element_type=jnp.float32
            ).astype(jnp.bfloat16)
            outgoing[pl.ds(group * 4 * CAP, 4 * CAP), cols] = block
            if group == 0:
                arrived[pl.ds(0, CAP), cols] = block[:CAP]
            return carry

        lax.fori_loop(0, 4, place_columns, 0)
        for p in range(max(1, group * 4), group * 4 + 4):
            disp_copy(p).start()

    arrivals(1, *set_one)

    route = route_ref[...]
    slot_rows = lax.broadcasted_iota(jnp.int32, (EXPERTS * CAP, tokens), 0)
    weighted = jnp.where(slot_rows == slots[0], route[0:1, :], 0.0) + jnp.where(
        slot_rows == slots[1], route[1:2, :], 0.0
    )
    picking[...] = weighted.T.astype(jnp.bfloat16)

    halo_copy.wait_recv()
    row_count = pool_in.shape[1]
    window_group = (tp * 64) // GROUP_CH
    gain_wide = pool_gain[...]
    diagonal = lax.broadcasted_iota(jnp.int32, (64, 64), 0) == lax.broadcasted_iota(
        jnp.int32, (64, 64), 1
    )
    gain_col = jnp.sum(jnp.where(diagonal, gain_wide, 0.0), axis=1, keepdims=True)
    for part in range(4):
        r = slice(part * 16, part * 16 + 16)
        values = pool_in[r, :].astype(jnp.float32)
        carried = jnp.where(ep > 0, halo[r, :].astype(jnp.float32), 0.0)
        level = jnp.concatenate([carried, values], axis=1)
        summed = jnp.zeros_like(values)
        for doubling in range(4):
            level = level + pltpu.roll(level, 2**doubling, 1)
            summed = jnp.where(window_group == doubling, level[:, 128:], summed)
        position = ep * row_count + lax.broadcasted_iota(jnp.int32, (1, row_count), 1)
        width = 2 ** 1
        for doubling in range(1, 4):
            width = jnp.where(window_group == doubling, 2 ** (doubling + 1), width)
        counted = jnp.minimum(position + 1, width).astype(jnp.float32)
        pooled[r, :] = ((summed / counted - values) * gain_col[r, :]).astype(jnp.bfloat16)
    pooled_all[pl.ds(0, 64), :] = pooled[:, pl.ds(pl.multiple_of(tp * 128, 128), 128)]

    def pool_copy(dz, dc):
        target = lax.rem(pz + dz, NZ) * 2 + lax.rem(core + dc, 2)
        rel = -dz if dz <= 4 else NZ - dz
        return pltpu.make_async_remote_copy(
            src_ref=pooled.at[:, pl.ds(pl.multiple_of(target * 128, 128), 128)],
            dst_ref=pooled_all.at[pl.ds(SLOT_OF[rel] * 128 + 64 * dc, 64)],
            send_sem=pool_sem.at[0],
            recv_sem=pool_sem.at[1],
            device_id=column(dz, dc),
            device_id_type=DEV,
        )

    half_rows = 8 * CAP

    def expert_chunk(half, chunk):
        rows = pl.ds(pl.multiple_of(half * half_rows, half_rows), half_rows)
        cols = pl.ds(pl.multiple_of(chunk * 256, 256), 256)
        r = arrived[rows, :]
        dims = (((1,), (1,)), ((), ()))
        gate_part = lax.dot_general(r, w_gate[cols, :], dims, preferred_element_type=jnp.float32)
        upward = lax.dot_general(r, w_up[cols, :], dims, preferred_element_type=jnp.float32)
        act = gate_part / (1.0 + jnp.exp(-gate_part)) * upward
        hidden[rows, cols] = act.astype(jnp.bfloat16)

    def expert_chunks(half, begin, end):
        def one(chunk, carry):
            expert_chunk(half, chunk)
            return carry

        lax.fori_loop(begin, end, one, 0)

    def ret_copy(q, p):
        dx, dy = OFFSETS[p]
        rows = pl.ds(p * CAP, CAP)
        return pltpu.make_async_remote_copy(
            src_ref=rows_out.at[q, rows],
            dst_ref=rows_back.at[q, rows],
            send_sem=ret_send.at[q],
            recv_sem=ret_recv.at[q],
            device_id=plane(NX - dx, NY - dy),
            device_id_type=DEV,
        )

    def give_back(q):
        wait_for(w_down.at[q, pl.ds(0, 512)], sib_down.at[q])
        for half in range(2):
            rows = pl.ds(half * half_rows, half_rows)
            block = jnp.dot(
                hidden[rows, :], w_down[q], preferred_element_type=jnp.float32
            ).astype(jnp.bfloat16)
            rows_out[q, rows] = block
            if half == 0:
                rows_back[q, pl.ds(0, CAP)] = block[:CAP]
            for p in range(max(1, half * 8), half * 8 + 8):
                ret_copy(q, p).start()

    def moe_store(q):
        cols = pl.ds(q * 512, 512)
        return pltpu.make_async_copy(moe_vmem.at[q], moe_hbm.at[:, cols], store_sem.at[q])

    def combine(q):
        wait_for(rows_back.at[q, pl.ds(CAP, 15 * CAP)], ret_recv.at[q])
        moe_vmem[q] = jnp.dot(
            picking[...], rows_back[q], preferred_element_type=jnp.float32
        ).astype(jnp.bfloat16)
        moe_store(q).start()

    arrivals(2, *set_one)

    wait_for(arrived.at[pl.ds(CAP, 7 * CAP)], disp_recv.at[0])
    wait_for(w_gate.at[pl.ds(0, 256)], sib_gate.at[0])
    wait_for(w_up.at[pl.ds(0, 256)], sib_up.at[0])
    expert_chunks(0, 0, 2)

    arrivals(3, *set_one)
    for q in range(1, 4):
        loads[f"d{q}"].wait()
    first_sends(*set_two)
    for q in range(1, 4):
        push(f"d{q}", 0)
    wait_for(w_gate.at[pl.ds(0, 128)], sib_gate.at[1])
    wait_for(w_up.at[pl.ds(0, 128)], sib_up.at[1])
    expert_chunks(0, 2, 3)
    wait_for(arrived.at[pl.ds(8 * CAP, 8 * CAP)], disp_recv.at[1])
    expert_chunks(1, 0, 3)
    arrivals(4, *set_one)
    arrivals(1, *set_two)
    wait_for(w_gate.at[pl.ds(0, 128)], sib_gate.at[2])
    wait_for(w_up.at[pl.ds(0, 128)], sib_up.at[2])
    expert_chunks(0, 3, 4)
    expert_chunks(1, 3, 4)
    give_back(0)
    arrivals(2, *set_two)
    arrivals(3, *set_two)
    for dz in (4, 3, 5, 2, 6, 1, 7, 0):
        for dc in range(2):
            if (dz, dc) != (0, 0):
                pool_copy(dz, dc).start()
    for h in range(2):
        loads[f"m{h}"].wait()
    first_sends(*set_mix)
    for h in range(2):
        push(f"m{h}", 0)
    arrivals(4, *set_two)
    give_back(1)
    give_back(2)
    give_back(3)
    arrivals(1, *set_mix)
    combine(0)
    arrivals(2, *set_mix)
    combine(1)
    arrivals(3, *set_mix)
    combine(2)
    arrivals(4, *set_mix)

    wait_for(pooled_all.at[pl.ds(64, 960)], pool_sem.at[1])
    pooled_rows = pooled_all[...].astype(jnp.float32).T.astype(jnp.bfloat16)
    for h in range(2):
        wait_for(w_mix.at[h, pl.ds(0, 512)], sib_mix.at[h])
        mixed_vmem[h] = jnp.dot(
            pooled_rows, w_mix[h], preferred_element_type=jnp.float32
        ).astype(jnp.bfloat16)
        pltpu.make_async_copy(
            mixed_vmem.at[h], mixed_hbm.at[:, pl.ds(h * 1024, 1024)], store_sem.at[4 + h]
        ).start()
    combine(3)

    for name in names:
        whole = span[name]
        wait_for(whole.at[pl.ds(0, 7 * 64)], ring_send.at[number[name]])
        wait_for(whole.at[pl.ds(0, 8 * 64)], push_send.at[number[name]])
    wait_for(outgoing.at[pl.ds(CAP, 15 * CAP)], disp_send)
    halo_copy.wait_send()
    wait_for(pooled_all.at[pl.ds(64, 960)], pool_sem.at[0])
    for q in range(4):
        wait_for(rows_out.at[q, pl.ds(CAP, 15 * CAP)], ret_send.at[q])
        moe_store(q).wait()
    for h in range(2):
        pltpu.make_async_copy(
            mixed_vmem.at[h], mixed_hbm.at[:, pl.ds(h * 1024, 1024)], store_sem.at[4 + h]
        ).wait()


def body(
    pool_input,
    pool_gain,
    mix_weight,
    moe_input,
    moe_gain,
    expert_ids,
    route_weight,
    gate_weight,
    up_weight,
    down_weight,
):
    rows_a, channels = pool_input.shape
    tokens, width = moe_input.shape
    slots = EXPERTS * CAP
    bf, f32 = jnp.bfloat16, jnp.float32
    hbm = pl.BlockSpec(memory_space=pl.ANY)
    vmem = pl.BlockSpec(memory_space=pltpu.VMEM)
    dma = pltpu.SemaphoreType.DMA
    return pl.pallas_call(
        kernel,
        out_shape=(
            jax.ShapeDtypeStruct((rows_a // 16, width), bf),
            jax.ShapeDtypeStruct((tokens, width), bf),
        ),
        in_specs=[hbm] * 6 + [vmem] * 4,
        out_specs=(hbm, hbm),
        scratch_shapes=[
            pltpu.VMEM((1024, width), bf),
            pltpu.VMEM((1024, width), bf),
            pltpu.VMEM((4, 1024, 512), bf),
            pltpu.VMEM((2, 1024, 1024), bf),
            pltpu.VMEM((channels, rows_a), bf),
            pltpu.VMEM((channels, 128), bf),
            pltpu.VMEM((channels, rows_a), bf),
            pltpu.VMEM((1024, 128), bf),
            pltpu.VMEM((tokens, width), bf),
            pltpu.VMEM((tokens, width), bf),
            pltpu.VMEM((4 * CAP, tokens), bf),
            pltpu.VMEM((tokens, slots), bf),
            pltpu.VMEM((slots, width), bf),
            pltpu.VMEM((slots, width), bf),
            pltpu.VMEM((slots, 1024), bf),
            pltpu.VMEM((4, slots, 512), bf),
            pltpu.VMEM((4, slots, 512), bf),
            pltpu.VMEM((4, tokens, 512), bf),
            pltpu.VMEM((2, rows_a // 16, 1024), bf),
            dma((10,)),
            dma((6,)),
            dma((8, 8)),
            dma((8,)),
            dma((8,)),
            dma((3,)),
            dma((3,)),
            dma((4,)),
            dma((2,)),
            dma,
            dma((2,)),
            dma((2,)),
            dma((2,)),
            dma((4,)),
            dma((4,)),
        ],
        compiler_params=pltpu.CompilerParams(
            collective_id=0, has_side_effects=True, vmem_limit_bytes=60 << 20
        ),
        name="mixer_and_experts",
    )(
        gate_weight[0].T,
        up_weight[0].T,
        down_weight[0].T,
        mix_weight,
        pool_input.T,
        moe_input,
        pool_gain.reshape(1, channels),
        moe_gain.reshape(1, width),
        expert_ids.T,
        route_weight.T,
    )


def solution(mesh):
    return jax.shard_map(
        body,
        mesh=mesh,
        in_specs=(
            P("ep", "tp"),
            P("tp"),
            P("tp", None),
            P(("ep", "tp"), None),
            P(),
            P(("ep", "tp"), None),
            P(("ep", "tp"), None),
            P("ep", None, "tp"),
            P("ep", None, "tp"),
            P("ep", None, "tp"),
        ),
        out_specs=(P(("ep", "tp"), None), P(("ep", "tp"), None)),
        check_vma=False,
    )
```

time: 170 us -> 113 us (0.66)
  Pallas kernels: 0 us -> 109 us
  blocking collectives: 74.3 us -> 0 us
  waiting for transfers between devices: 38.6 us -> 0 us
  matrix products: 23.6 us -> 0 us
  between operations: 14.3 us -> 0.65 us
  starting transfers between devices: 7.71 us -> 0 us
  other arithmetic: 5.79 us -> 0 us
    pallas_call x0 -> x1, Pallas kernels: none -> 109 us  [body(): pl.pallas_call(kernel, out_shape=(jax.ShapeDtypeStruct((rows_a // 16, wid...]
    all_to_all x2 -> x0, blocking collectives: 74.3 us -> none  [the longest x1 45.8 us: body(): lax.all_to_all(outgoing, 'ep', split_axis=0, concat_axis=1, tiled=True)]
    dot_general x7 -> x0, matrix products: 23.6 us -> none  [the longest x1 6.39 us: body(): jnp.dot(pooled, mix_weight, preferred_element_type=jnp.float32)]
    all_to_all x1 -> x0, waiting for transfers between devices: 20.9 us -> none  [exchange_in_pieces(): lax.all_to_all(section, axis, split_axis=0, concat_axis=0, tiled=True)]
    all_gather x1 -> x0, waiting for transfers between devices: 16.9 us -> none  [gather_turned(): lax.all_gather(both, axis, axis=0, tiled=True)]
    ppermute x1 -> x0, starting transfers between devices: 3.92 us -> none  [from_behind(): return lax.ppermute(shard, axis, pairs)]
    all_to_all x1 -> x0, starting transfers between devices: 3.71 us -> none  [exchange_in_pieces(): lax.all_to_all(section, axis, split_axis=0, concat_axis=0, tiled=True)]
    concatenate x2 -> x0, other arithmetic: 2.43 us -> none  [the longest x1 2.07 us: gather_turned(): both = jnp.concatenate([t.reshape(len(t), -1) for t in turned], axis=1)]
  transfers between devices with their start and end apart: 4 -> 0, of which waited for: 3 -> 0; matrix products, arithmetic and copies ran while one was open for 18% -> 0% of each run, Pallas kernels for 0% -> 0%
where the time goes in v1:
time: 113 us; the launch traced here: 112 us
  Pallas kernels  109 us (96%)
  local copies, waits for them, and re-layouts  2.94 us (3%)
    pallas_call x1, Pallas kernels, body(): pl.pallas_call(kernel, out_shape=(jax.ShapeDtypeStruct((rows_a // 16, wid...  109 us
    unnamed x4, local copies, waits for them, and re-layouts  2.94 us

profile of v1, /device:TPU:1, one launch (start us, length us, event | category | flops | bytes accessed | tf_op | source)
XLA Modules:
  0.0 112.5 jit_solution(14942925564953531450)
XLA Ops:
  0.6 108.9 %mixer_and_experts.1 = (bf16[128,2048]{1,0:T(8,128)(2,1)}, bf16[256,2048]{1,0:T(8,128)(2,1)}) custom-call(bf16[64,2048]{1,0:T(8,128)(2,1)} %bitcast.14, bf16[64,2048]{1,0:T(8,128)(2,1)} %bitcast.15, bf16[64,2048]{1,0:T(8,128)(2,1)} %bitcast.16, bf16[64,2048]{1,0:T(8,128)(2,1)} %mix_hbm.1, bf16[64,2048]{1,0:T(8,128)(2,1)} %bitcast.17, ...), custom_call_target="tpu_custom_call" | custom-call | tf_op jit(solution)/shard_map/mixer_and_experts/pallas_call | solution.py:433
  109.5 0.0 copy-start
  109.5 2.0 %copy.14 = bf16[128,2048]{1,0:T(8,128)(2,1)} copy(bf16[128,2048]{1,0:T(8,128)(2,1)} %get-tuple-element.4) | data formatting | bytes 1048576
  111.5 0.0 copy-done
  111.5 1.0 copy.15
Async XLA Ops:
  109.5 2.0 %copy-start = (bf16[256,2048]{1,0:T(8,128)(2,1)S(1)}, bf16[256,2048]{1,0:T(8,128)(2,1)}, u32[]{:S(2)}) copy-start(bf16[256,2048]{1,0:T(8,128)(2,1)} %get-tuple-element.5) | copy-start | bytes 3145732

commit v2 on v1

--- a/solution.py
+++ b/solution.py
@@ -22,6 +22,9 @@
 CW, CCW = 0, 1
 
 
+phase = jax.named_scope
+
+
 def wait_for(ref, sem):
     pltpu.make_async_copy(ref, ref, sem).wait()
 
@@ -29,11 +32,11 @@
 def kernel(
     gate_hbm, up_hbm, down_hbm, mix_hbm, pool_hbm, x_hbm,
     pool_gain, moe_gain, ids_ref, route_ref,
-    mixed_hbm, moe_hbm,
-    w_gate, w_up, w_down, w_mix,
+    mixed_ref, moe_ref,
+    w_in, w_down, w_mix,
     pool_in, halo, pooled, pooled_all, x_in, normed, placing, picking,
-    outgoing, arrived, hidden, rows_out, rows_back, moe_vmem, mixed_vmem,
-    load_sem, store_sem, ring_recv, ring_send, push_send, sib_gate, sib_up, sib_down, sib_mix,
+    outgoing, arrived, hidden, rows_out, rows_back, pooled_rows, mixed_sum,
+    load_sem, ring_recv, ring_send, push_send, sib_in, sib_down, sib_mix,
     disp_send, disp_recv, halo_sem, pool_sem, ret_send, ret_recv,
 ):
     ep = lax.axis_index("ep")
@@ -65,17 +68,17 @@
 
         return at
 
-    pieces = {"g": piece(w_gate), "u": piece(w_up)}
+    pieces = {
+        "g": lambda slot, other: w_in.at[slot, pl.ds(64 * other, 64)],
+        "u": lambda slot, other: w_in.at[slot, pl.ds(128 + 64 * other, 64)],
+    }
     hops = {"g": (4, 3), "u": (3, 4)}
-    span = {"g": w_gate, "u": w_up}
     for q in range(4):
         pieces[f"d{q}"] = piece(w_down, q)
         hops[f"d{q}"] = (4, 3) if q % 2 == 0 else (3, 4)
-        span[f"d{q}"] = w_down.at[q]
     for h in range(2):
         pieces[f"m{h}"] = piece(w_mix, h)
         hops[f"m{h}"] = (4, 3) if h == 0 else (3, 4)
-        span[f"m{h}"] = w_mix.at[h]
     names = list(pieces)
     number = {name: k for k, name in enumerate(names)}
 
@@ -86,8 +89,8 @@
         copy.start()
         loads[name] = copy
 
-    load("g", gate_hbm, w_gate.at[pl.ds(0, 64)])
-    load("u", up_hbm, w_up.at[pl.ds(0, 64)])
+    load("g", gate_hbm, w_in.at[0, pl.ds(0, 64)])
+    load("u", up_hbm, w_in.at[0, pl.ds(128, 64)])
     load("d0", down_hbm.at[:, pl.ds(0, 512)], w_down.at[0, pl.ds(0, 64)])
     load("x", x_hbm, x_in)
     load("pool", pool_hbm, pool_in)
@@ -97,13 +100,11 @@
         load(f"m{h}", mix_hbm.at[:, pl.ds(1024 * h, 1024)], w_mix.at[h, pl.ds(0, 64)])
 
     def sib_sem(name, slot):
-        if name == "g":
-            return sib_gate.at[(0, 0, 0, 0, 1, 1, 2, 2)[slot]]
-        if name == "u":
-            return sib_up.at[(0, 0, 0, 0, 1, 1, 2, 2)[slot]]
+        if name in "gu":
+            return sib_in.at[number[name], (0, 0, 0, 1, 1, 2, 2, 3)[slot]]
         if name[0] == "d":
             return sib_down.at[int(name[1])]
-        return sib_mix.at[int(name[1])]
+        return sib_mix.at[int(name[1]), slot // 7]
 
     def ring_copy(name, way, hop):
         sign = -1 if way == CW else 1
@@ -146,17 +147,20 @@
             arrival(name, way, hop)
 
     set_one = (("g", CW), ("u", CCW), ("u", CW), ("g", CCW), ("d0", CW), ("d0", CCW))
-    set_two = tuple((f"d{q}", way) for q in (1, 2, 3) for way in (CCW, CW))
     set_mix = (("m0", CW), ("m1", CCW), ("m1", CW), ("m0", CCW))
 
-    pl.semaphore_wait(barrier, 30)
-
-    loads["g"].wait()
-    first_sends(("g", CW))
-    loads["u"].wait()
-    first_sends(*set_one[1:4])
-    loads["d0"].wait()
-    first_sends(*set_one[4:])
+    def both(name):
+        return ((name, CCW), (name, CW))
+
+    with phase("enter"):
+        pl.semaphore_wait(barrier, 30)
+    with phase("first"):
+        loads["g"].wait()
+        first_sends(("g", CW))
+        loads["u"].wait()
+        first_sends(*set_one[1:4])
+        loads["d0"].wait()
+        first_sends(*set_one[4:])
 
     loads["pool"].wait()
     halo_copy = pltpu.make_async_remote_copy(
@@ -182,7 +186,8 @@
         normed[rows, :] = (v * scale * gain_row).astype(jnp.bfloat16)
         return carry
 
-    lax.fori_loop(0, 4, norm_rows, 0)
+    with phase("norm"):
+        lax.fori_loop(0, 4, norm_rows, 0)
 
     tokens = x_in.shape[0]
     expert = lax.broadcasted_iota(jnp.int32, (EXPERTS, tokens), 0)
@@ -210,7 +215,7 @@
             src_ref=outgoing.at[rows],
             dst_ref=arrived.at[rows],
             send_sem=disp_send,
-            recv_sem=disp_recv.at[0 if p < 8 else 1],
+            recv_sem=disp_recv.at[p // 8],
             device_id=plane(dx, dy),
             device_id_type=DEV,
         )
@@ -231,10 +236,17 @@
             return carry
 
         lax.fori_loop(0, 4, place_columns, 0)
-        for p in range(max(1, group * 4), group * 4 + 4):
-            disp_copy(p).start()
-
-    arrivals(1, *set_one)
+        if group < 2:
+            for p in range(max(1, group * 4), group * 4 + 4):
+                disp_copy(p).start()
+
+    with phase("one_1"):
+        arrivals(1, *set_one)
+    for p in range(8, 16):
+        disp_copy(p).start()
+    loads["d1"].wait()
+    first_sends(*both("d1"))
+    push("d1", 0)
 
     route = route_ref[...]
     slot_rows = lax.broadcasted_iota(jnp.int32, (EXPERTS * CAP, tokens), 0)
@@ -243,7 +255,8 @@
     )
     picking[...] = weighted.T.astype(jnp.bfloat16)
 
-    halo_copy.wait_recv()
+    with phase("halo"):
+        halo_copy.wait_recv()
     row_count = pool_in.shape[1]
     window_group = (tp * 64) // GROUP_CH
     gain_wide = pool_gain[...]
@@ -282,22 +295,27 @@
 
     half_rows = 8 * CAP
 
-    def expert_chunk(half, chunk):
-        rows = pl.ds(pl.multiple_of(half * half_rows, half_rows), half_rows)
-        cols = pl.ds(pl.multiple_of(chunk * 256, 256), 256)
-        r = arrived[rows, :]
-        dims = (((1,), (1,)), ((), ()))
-        gate_part = lax.dot_general(r, w_gate[cols, :], dims, preferred_element_type=jnp.float32)
-        upward = lax.dot_general(r, w_up[cols, :], dims, preferred_element_type=jnp.float32)
-        act = gate_part / (1.0 + jnp.exp(-gate_part)) * upward
-        hidden[rows, cols] = act.astype(jnp.bfloat16)
-
-    def expert_chunks(half, begin, end):
-        def one(chunk, carry):
-            expert_chunk(half, chunk)
+    def gated(both_parts):
+        gate_part, upward = both_parts[:, :128], both_parts[:, 128:]
+        return (gate_part / (1.0 + jnp.exp(-gate_part)) * upward).astype(jnp.bfloat16)
+
+    def project(rows, weights):
+        return lax.dot_general(
+            arrived[rows, :], weights, (((1,), (1,)), ((), ())), preferred_element_type=jnp.float32
+        )
+
+    def hidden_pairs(half, first_slot, pairs):
+        rows = pl.ds(half * half_rows, half_rows)
+
+        def one(pair, carry):
+            slot = first_slot + 2 * pair
+            sums = project(rows, w_in[pl.ds(slot, 2)].reshape(512, w_in.shape[2]))
+            for k in range(2):
+                cols = pl.ds(pl.multiple_of((slot + k) * 128, 128), 128)
+                hidden[rows, cols] = gated(sums[:, 256 * k : 256 * k + 256])
             return carry
 
-        lax.fori_loop(begin, end, one, 0)
+        lax.fori_loop(0, pairs, one, 0)
 
     def ret_copy(q, p):
         dx, dy = OFFSETS[p]
@@ -311,104 +329,164 @@
             device_id_type=DEV,
         )
 
-    def give_back(q):
-        wait_for(w_down.at[q, pl.ds(0, 512)], sib_down.at[q])
-        for half in range(2):
-            rows = pl.ds(half * half_rows, half_rows)
-            block = jnp.dot(
-                hidden[rows, :], w_down[q], preferred_element_type=jnp.float32
-            ).astype(jnp.bfloat16)
-            rows_out[q, rows] = block
-            if half == 0:
-                rows_back[q, pl.ds(0, CAP)] = block[:CAP]
-            for p in range(max(1, half * 8), half * 8 + 8):
-                ret_copy(q, p).start()
-
-    def moe_store(q):
-        cols = pl.ds(q * 512, 512)
-        return pltpu.make_async_copy(moe_vmem.at[q], moe_hbm.at[:, cols], store_sem.at[q])
+    def give_back(q, half):
+        rows = pl.ds(half * half_rows, half_rows)
+        block = jnp.dot(
+            hidden[rows, :], w_down[q], preferred_element_type=jnp.float32
+        ).astype(jnp.bfloat16)
+        rows_out[q, rows] = block
+        if half == 0:
+            rows_back[q, pl.ds(0, CAP)] = block[:CAP]
+        for p in range(max(1, half * 8), half * 8 + 8):
+            ret_copy(q, p).start()
 
     def combine(q):
         wait_for(rows_back.at[q, pl.ds(CAP, 15 * CAP)], ret_recv.at[q])
-        moe_vmem[q] = jnp.dot(
+        moe_ref[:, pl.ds(q * 512, 512)] = jnp.dot(
             picking[...], rows_back[q], preferred_element_type=jnp.float32
         ).astype(jnp.bfloat16)
-        moe_store(q).start()
-
-    arrivals(2, *set_one)
-
-    wait_for(arrived.at[pl.ds(CAP, 7 * CAP)], disp_recv.at[0])
-    wait_for(w_gate.at[pl.ds(0, 256)], sib_gate.at[0])
-    wait_for(w_up.at[pl.ds(0, 256)], sib_up.at[0])
-    expert_chunks(0, 0, 2)
-
-    arrivals(3, *set_one)
-    for q in range(1, 4):
+
+    def down_ready(q):
+        wait_for(w_down.at[q, pl.ds(0, 512)], sib_down.at[q])
+
+    def in_ready(hop):
+        for part in range(2):
+            if hop == 1:
+                wait_for(arrived.at[pl.ds(0, 192)], sib_in.at[part, 0])
+            else:
+                wait_for(w_in.at[0, pl.ds(0, 64 if hop == 4 else 128)], sib_in.at[part, hop - 1])
+
+    with phase("in_1"):
+        in_ready(1)
+    with phase("one_2"):
+        arrivals(2, *set_one)
+    with phase("d1_1"):
+        arrivals(1, *both("d1"))
+    with phase("disp_0"):
+        wait_for(arrived.at[pl.ds(CAP, 7 * CAP)], disp_recv.at[0])
+        in_ready(2)
+    with phase("hid_a"):
+        hidden_pairs(0, 0, 2)
+    with phase("one_3"):
+        arrivals(3, *set_one)
+    with phase("d1_2"):
+        arrivals(2, *both("d1"))
+    for q in (2, 3):
         loads[f"d{q}"].wait()
-    first_sends(*set_two)
-    for q in range(1, 4):
+        first_sends(*both(f"d{q}"))
         push(f"d{q}", 0)
-    wait_for(w_gate.at[pl.ds(0, 128)], sib_gate.at[1])
-    wait_for(w_up.at[pl.ds(0, 128)], sib_up.at[1])
-    expert_chunks(0, 2, 3)
-    wait_for(arrived.at[pl.ds(8 * CAP, 8 * CAP)], disp_recv.at[1])
-    expert_chunks(1, 0, 3)
-    arrivals(4, *set_one)
-    arrivals(1, *set_two)
-    wait_for(w_gate.at[pl.ds(0, 128)], sib_gate.at[2])
-    wait_for(w_up.at[pl.ds(0, 128)], sib_up.at[2])
-    expert_chunks(0, 3, 4)
-    expert_chunks(1, 3, 4)
-    give_back(0)
-    arrivals(2, *set_two)
-    arrivals(3, *set_two)
+    with phase("in_3"):
+        in_ready(3)
+    with phase("hid_b"):
+        hidden_pairs(0, 4, 1)
+    with phase("disp_1"):
+        wait_for(arrived.at[pl.ds(8 * CAP, 8 * CAP)], disp_recv.at[1])
+    with phase("hid_c"):
+        hidden_pairs(1, 0, 3)
+    with phase("one_4"):
+        arrivals(4, *set_one[:4])
+    with phase("one_4d"):
+        arrivals(4, *set_one[4:])
+    with phase("in_4"):
+        in_ready(4)
+    with phase("hid_67a"):
+        hidden_pairs(0, 6, 1)
+    with phase("d0"):
+        down_ready(0)
+    with phase("give_0a"):
+        give_back(0, 0)
+    with phase("hid_67b"):
+        hidden_pairs(1, 6, 1)
+    with phase("give_0b"):
+        give_back(0, 1)
+    with phase("two_1"):
+        arrivals(3, *both("d1"))
+        arrivals(1, *both("d2"))
+        arrivals(1, *both("d3"))
+    with phase("two_2"):
+        arrivals(4, *both("d1"))
+        arrivals(2, *both("d2"))
+        arrivals(2, *both("d3"))
+    for h in range(2):
+        loads[f"m{h}"].wait()
+    first_sends(*set_mix[:2])
+    with phase("d1"):
+        down_ready(1)
+    with phase("give_1"):
+        give_back(1, 0)
+        give_back(1, 1)
+    with phase("two_3"):
+        arrivals(3, *both("d2"))
+        arrivals(3, *both("d3"))
+    first_sends(*set_mix[2:])
+    for h in range(2):
+        push(f"m{h}", 0)
     for dz in (4, 3, 5, 2, 6, 1, 7, 0):
         for dc in range(2):
             if (dz, dc) != (0, 0):
                 pool_copy(dz, dc).start()
+    with phase("mix_1a"):
+        arrivals(1, *set_mix[:2])
+    with phase("two_4"):
+        arrivals(4, *both("d2"))
+        arrivals(4, *both("d3"))
+    with phase("d2"):
+        down_ready(2)
+    with phase("give_2"):
+        give_back(2, 0)
+        give_back(2, 1)
+    with phase("d3"):
+        down_ready(3)
+    with phase("give_3"):
+        give_back(3, 0)
+        give_back(3, 1)
+    with phase("mix_1b"):
+        arrivals(1, *set_mix[2:])
+    with phase("combine_0"):
+        combine(0)
+    with phase("mix_2"):
+        arrivals(2, *set_mix)
+    with phase("combine_1"):
+        combine(1)
+    with phase("pool_wait"):
+        wait_for(pooled_all.at[pl.ds(64, 960)], pool_sem.at[1])
+    pooled_rows[...] = pooled_all[...].astype(jnp.float32).T.astype(jnp.bfloat16)
+    with phase("mix_3"):
+        arrivals(3, *set_mix)
+
     for h in range(2):
-        loads[f"m{h}"].wait()
-    first_sends(*set_mix)
-    for h in range(2):
-        push(f"m{h}", 0)
-    arrivals(4, *set_two)
-    give_back(1)
-    give_back(2)
-    give_back(3)
-    arrivals(1, *set_mix)
-    combine(0)
-    arrivals(2, *set_mix)
-    combine(1)
-    arrivals(3, *set_mix)
-    combine(2)
-    arrivals(4, *set_mix)
-
-    wait_for(pooled_all.at[pl.ds(64, 960)], pool_sem.at[1])
-    pooled_rows = pooled_all[...].astype(jnp.float32).T.astype(jnp.bfloat16)
-    for h in range(2):
-        wait_for(w_mix.at[h, pl.ds(0, 512)], sib_mix.at[h])
-        mixed_vmem[h] = jnp.dot(
-            pooled_rows, w_mix[h], preferred_element_type=jnp.float32
-        ).astype(jnp.bfloat16)
-        pltpu.make_async_copy(
-            mixed_vmem.at[h], mixed_hbm.at[:, pl.ds(h * 1024, 1024)], store_sem.at[4 + h]
-        ).start()
-    combine(3)
+        wait_for(w_mix.at[h, pl.ds(0, 448)], sib_mix.at[h, 0])
+    with phase("mixer"):
+        for h in range(2):
+            mixed_sum[h] = jnp.dot(
+                pooled_rows[:, :896], w_mix[h, :896], preferred_element_type=jnp.float32
+            )
+    with phase("combine_2"):
+        combine(2)
+    with phase("mix_4"):
+        arrivals(4, *set_mix)
+        for h in range(2):
+            wait_for(w_mix.at[h, pl.ds(0, 64)], sib_mix.at[h, 1])
+    with phase("mixer_2"):
+        for h in range(2):
+            last = jnp.dot(pooled_rows[:, 896:], w_mix[h, 896:], preferred_element_type=jnp.float32)
+            mixed_ref[:, pl.ds(h * 1024, 1024)] = (mixed_sum[h] + last).astype(jnp.bfloat16)
+    with phase("combine_3"):
+        combine(3)
 
     for name in names:
-        whole = span[name]
-        wait_for(whole.at[pl.ds(0, 7 * 64)], ring_send.at[number[name]])
-        wait_for(whole.at[pl.ds(0, 8 * 64)], push_send.at[number[name]])
+        if name in "gu":
+            sent, pushed = outgoing.at[pl.ds(0, 7 * 64)], outgoing.at[pl.ds(0, 8 * 64)]
+        else:
+            whole = w_down.at[int(name[1])] if name[0] == "d" else w_mix.at[int(name[1])]
+            sent, pushed = whole.at[pl.ds(0, 7 * 64)], whole.at[pl.ds(0, 8 * 64)]
+        wait_for(sent, ring_send.at[number[name]])
+        wait_for(pushed, push_send.at[number[name]])
     wait_for(outgoing.at[pl.ds(CAP, 15 * CAP)], disp_send)
     halo_copy.wait_send()
     wait_for(pooled_all.at[pl.ds(64, 960)], pool_sem.at[0])
     for q in range(4):
         wait_for(rows_out.at[q, pl.ds(CAP, 15 * CAP)], ret_send.at[q])
-        moe_store(q).wait()
-    for h in range(2):
-        pltpu.make_async_copy(
-            mixed_vmem.at[h], mixed_hbm.at[:, pl.ds(h * 1024, 1024)], store_sem.at[4 + h]
-        ).wait()
 
 
 def body(
@@ -433,14 +511,13 @@
     return pl.pallas_call(
         kernel,
         out_shape=(
-            jax.ShapeDtypeStruct((rows_a // 16, width), bf),
-            jax.ShapeDtypeStruct((tokens, width), bf),
+            pltpu.VMEM((rows_a // 16, width), bf),
+            pltpu.VMEM((tokens, width), bf),
         ),
         in_specs=[hbm] * 6 + [vmem] * 4,
-        out_specs=(hbm, hbm),
+        out_specs=(vmem, vmem),
         scratch_shapes=[
-            pltpu.VMEM((1024, width), bf),
-            pltpu.VMEM((1024, width), bf),
+            pltpu.VMEM((8, 256, width), bf),
             pltpu.VMEM((4, 1024, 512), bf),
             pltpu.VMEM((2, 1024, 1024), bf),
             pltpu.VMEM((channels, rows_a), bf),
@@ -456,17 +533,15 @@
             pltpu.VMEM((slots, 1024), bf),
             pltpu.VMEM((4, slots, 512), bf),
             pltpu.VMEM((4, slots, 512), bf),
-            pltpu.VMEM((4, tokens, 512), bf),
-            pltpu.VMEM((2, rows_a // 16, 1024), bf),
+            pltpu.VMEM((rows_a // 16, 1024), bf),
+            pltpu.VMEM((2, rows_a // 16, 1024), f32),
             dma((10,)),
-            dma((6,)),
             dma((8, 8)),
             dma((8,)),
             dma((8,)),
-            dma((3,)),
-            dma((3,)),
+            dma((2, 4)),
             dma((4,)),
-            dma((2,)),
+            dma((2, 2)),
             dma,
             dma((2,)),
             dma((2,)),
@@ -475,7 +550,7 @@
             dma((4,)),
         ],
         compiler_params=pltpu.CompilerParams(
-            collective_id=0, has_side_effects=True, vmem_limit_bytes=60 << 20
+            collective_id=0, has_side_effects=True, vmem_limit_bytes=56 << 20
         ),
         name="mixer_and_experts",
     )(

time: 113 us -> 110 us (0.973)
  Pallas kernels: 109 us -> 107 us
  local copies, waits for them, and re-layouts: 2.94 us -> 1.77 us
    pallas_call x1, Pallas kernels: 109 us -> 107 us  [body(): pl.pallas_call(kernel, out_shape=(pltpu.VMEM((rows_a // 16, width), bf),...]
    unnamed x4 -> x2, local copies, waits for them, and re-layouts: 2.94 us -> 1.77 us
where the time goes in v2:
time: 110 us; the launch traced here: 109 us
  Pallas kernels  107 us (97%)
  local copies, waits for them, and re-layouts  1.77 us (2%)
    pallas_call x1, Pallas kernels, body(): pl.pallas_call(kernel, out_shape=(pltpu.VMEM((rows_a // 16, width), bf),...  107 us

profile of v2, /device:TPU:1, one launch (start us, length us, event | category | flops | bytes accessed | tf_op | source)
XLA Modules:
  0.0 109.4 jit_solution(11789650628517168449)
XLA Ops:
  0.6 107.0 %mixer_and_experts.1 = (bf16[128,2048]{1,0:T(8,128)(2,1)S(1)}, bf16[256,2048]{1,0:T(8,128)(2,1)S(1)}) custom-call(bf16[64,2048]{1,0:T(8,128)(2,1)} %bitcast.14, bf16[64,2048]{1,0:T(8,128)(2,1)} %bitcast.15, bf16[64,2048]{1,0:T(8,128)(2,1)} %bitcast.16, bf16[64,2048]{1,0:T(8,128)(2,1)} %mix_hbm.1, bf16[64,2048]{1,0:T(8,128)(2,1)} %bitcast.17, ...), custom_call_target="tpu_custom_call" | custom-call | tf_op jit(solution)/shard_map/mixer_and_experts/pallas_call | solution.py:511
  107.6 0.8 copy.14
  108.4 1.0 copy.15

commit v3 on v2

--- a/solution.py
+++ b/solution.py
@@ -33,10 +33,10 @@
     gate_hbm, up_hbm, down_hbm, mix_hbm, pool_hbm, x_hbm,
     pool_gain, moe_gain, ids_ref, route_ref,
     mixed_ref, moe_ref,
-    w_in, w_down, w_mix,
+    w_in, w_down, w_mix, w_plane,
     pool_in, halo, pooled, pooled_all, x_in, normed, placing, picking,
     outgoing, arrived, hidden, rows_out, rows_back, pooled_rows, mixed_sum,
-    load_sem, ring_recv, ring_send, push_send, sib_in, sib_down, sib_mix,
+    load_sem, ring_recv, ring_send, push_send, sib_in, sib_down, sib_mix, plane_send, plane_recv,
     disp_send, disp_recv, halo_sem, pool_sem, ret_send, ret_recv,
 ):
     ep = lax.axis_index("ep")
@@ -97,7 +97,8 @@
     for q in range(1, 4):
         load(f"d{q}", down_hbm.at[:, pl.ds(512 * q, 512)], w_down.at[q, pl.ds(0, 64)])
     for h in range(2):
-        load(f"m{h}", mix_hbm.at[:, pl.ds(1024 * h, 1024)], w_mix.at[h, pl.ds(0, 64)])
+        load(f"m{h}", mix_hbm.at[:, pl.ds(1024 + 512 * h, 512)], w_mix.at[h, pl.ds(0, 64)])
+    load("plane", mix_hbm.at[:, pl.ds(0, 1024)], w_plane.at[0, pl.ds(0, 64)])
 
     def sib_sem(name, slot):
         if name in "gu":
@@ -119,11 +120,24 @@
             device_id_type=DEV,
         )
 
-    def push(name, slot):
+    def last_copy(name, half):
+        way = CW if name == "g" else CCW
+        at, rows = pieces[name], pl.ds(32 * half, 32)
+        source = SLOT_OF[-3 if way == CW else 3]
+        return pltpu.make_async_remote_copy(
+            src_ref=at(source, 0).at[rows],
+            dst_ref=at(SLOT_OF[4], 0).at[rows],
+            send_sem=ring_send.at[number[name]],
+            recv_sem=ring_recv.at[number[name], 3 + 4 * half],
+            device_id=ring_to[way],
+            device_id_type=DEV,
+        )
+
+    def push(name, slot, rows=slice(None)):
         at = pieces[name]
         pltpu.make_async_remote_copy(
-            src_ref=at(slot, 0),
-            dst_ref=at(slot, 1),
+            src_ref=at(slot, 0).at[rows],
+            dst_ref=at(slot, 1).at[rows],
             send_sem=push_send.at[number[name]],
             recv_sem=sib_sem(name, slot),
             device_id=sibling,
@@ -139,7 +153,11 @@
             return
         ring_copy(name, way, hop).wait_recv()
         if hop < hops[name][way]:
-            ring_copy(name, way, hop + 1).start()
+            if name in "gu" and hop == 3:
+                last_copy(name, 0).start()
+                last_copy(name, 1).start()
+            else:
+                ring_copy(name, way, hop + 1).start()
         push(name, SLOT_OF[-hop if way == CW else hop])
 
     def arrivals(hop, *pairs):
@@ -151,6 +169,45 @@
 
     def both(name):
         return ((name, CCW), (name, CW))
+
+    def plane_copy(number, source, target, device):
+        return pltpu.make_async_remote_copy(
+            src_ref=source,
+            dst_ref=target,
+            send_sem=plane_send.at[number],
+            recv_sem=plane_recv.at[number],
+            device_id=device,
+            device_id_type=DEV,
+        )
+
+    def x_part(at_x, first, count):
+        rows = pl.ds(pl.multiple_of(lax.rem(at_x, 2) * 32, 32), 32)
+        cols = pl.ds(pl.multiple_of((2 * py + at_x // 2) * 128, 128), 128)
+        return w_plane.at[pl.ds(first, count), rows, cols]
+
+    def y_part(at_y, first, count):
+        cols = pl.ds(pl.multiple_of(at_y * 256, 256), 256)
+        return w_plane.at[pl.ds(first, count), pl.ds(0, 64), cols]
+
+    x_own, y_own = x_part(px, 1, 7), y_part(py, 1, 7)
+    x_copies = [plane_copy(k, x_own, x_own, plane((0, 1, NX - 1, 2)[k], 0)) for k in (1, 2, 3)]
+    y_copies = [plane_copy(3 + k, y_own, y_own, plane(0, (0, 1, NY - 1, 2)[k])) for k in (1, 2, 3)]
+
+    def z_copy(dz):
+        rel = -dz if dz <= 4 else NZ - dz
+        own = x_part(px, 0, 1)
+        return plane_copy(0, own, x_part(px, SLOT_OF[rel], 1), column(dz, 0))
+
+    plane_pushes = [
+        plane_copy(
+            7 + k,
+            w_plane.at[pl.ds(k, (1, 7)[k]), pl.ds(0, 64)],
+            w_plane.at[pl.ds(k, (1, 7)[k]), pl.ds(64, 64)],
+            sibling,
+        )
+        for k in range(2)
+    ]
+    z_bytes = w_plane.at[pl.ds(1, 7), pl.ds(0, 32), pl.ds(0, 128)]
 
     with phase("enter"):
         pl.semaphore_wait(barrier, 30)
@@ -240,10 +297,12 @@
             for p in range(max(1, group * 4), group * 4 + 4):
                 disp_copy(p).start()
 
+    loads["plane"].wait()
+    for dz in (4, 3, 5, 2, 6, 1, 7):
+        z_copy(dz).start()
+    plane_pushes[0].start()
     with phase("one_1"):
         arrivals(1, *set_one)
-    for p in range(8, 16):
-        disp_copy(p).start()
     loads["d1"].wait()
     first_sends(*both("d1"))
     push("d1", 0)
@@ -358,8 +417,16 @@
 
     with phase("in_1"):
         in_ready(1)
-    with phase("one_2"):
-        arrivals(2, *set_one)
+    for p in range(8, 16):
+        disp_copy(p).start()
+    with phase("one_2a"):
+        arrivals(2, *set_one[:2])
+    with phase("plane_z"):
+        wait_for(z_bytes, plane_recv.at[0])
+    for copy in x_copies:
+        copy.start()
+    with phase("one_2b"):
+        arrivals(2, *set_one[2:])
     with phase("d1_1"):
         arrivals(1, *both("d1"))
     with phase("disp_0"):
@@ -369,22 +436,30 @@
         hidden_pairs(0, 0, 2)
     with phase("one_3"):
         arrivals(3, *set_one)
+    with phase("plane_x"):
+        for copy in x_copies:
+            copy.wait_recv()
+    for copy in y_copies:
+        copy.start()
+    with phase("in_3"):
+        in_ready(3)
+    with phase("hid_b"):
+        hidden_pairs(0, 4, 1)
     with phase("d1_2"):
         arrivals(2, *both("d1"))
     for q in (2, 3):
         loads[f"d{q}"].wait()
         first_sends(*both(f"d{q}"))
         push(f"d{q}", 0)
-    with phase("in_3"):
-        in_ready(3)
-    with phase("hid_b"):
-        hidden_pairs(0, 4, 1)
     with phase("disp_1"):
         wait_for(arrived.at[pl.ds(8 * CAP, 8 * CAP)], disp_recv.at[1])
     with phase("hid_c"):
         hidden_pairs(1, 0, 3)
     with phase("one_4"):
-        arrivals(4, *set_one[:4])
+        for half in range(2):
+            for name in "gu":
+                last_copy(name, half).wait_recv()
+                push(name, SLOT_OF[4], pl.ds(32 * half, 32))
     with phase("one_4d"):
         arrivals(4, *set_one[4:])
     with phase("in_4"):
@@ -406,27 +481,29 @@
     with phase("two_2"):
         arrivals(4, *both("d1"))
         arrivals(2, *both("d2"))
+        down_ready(1)
+    with phase("give_1a"):
+        give_back(1, 0)
+    with phase("two_2b"):
         arrivals(2, *both("d3"))
-    for h in range(2):
-        loads[f"m{h}"].wait()
-    first_sends(*set_mix[:2])
-    with phase("d1"):
-        down_ready(1)
-    with phase("give_1"):
-        give_back(1, 0)
+    for copy in y_copies:
+        copy.wait_recv()
+    plane_pushes[1].start()
+    with phase("give_1b"):
         give_back(1, 1)
     with phase("two_3"):
         arrivals(3, *both("d2"))
+    for h in range(2):
+        loads[f"m{h}"].wait()
+    with phase("two_3b"):
         arrivals(3, *both("d3"))
-    first_sends(*set_mix[2:])
+    first_sends(*set_mix)
     for h in range(2):
         push(f"m{h}", 0)
     for dz in (4, 3, 5, 2, 6, 1, 7, 0):
         for dc in range(2):
             if (dz, dc) != (0, 0):
                 pool_copy(dz, dc).start()
-    with phase("mix_1a"):
-        arrivals(1, *set_mix[:2])
     with phase("two_4"):
         arrivals(4, *both("d2"))
         arrivals(4, *both("d3"))
@@ -440,8 +517,8 @@
     with phase("give_3"):
         give_back(3, 0)
         give_back(3, 1)
-    with phase("mix_1b"):
-        arrivals(1, *set_mix[2:])
+    with phase("mix_1"):
+        arrivals(1, *set_mix)
     with phase("combine_0"):
         combine(0)
     with phase("mix_2"):
@@ -454,6 +531,15 @@
     with phase("mix_3"):
         arrivals(3, *set_mix)
 
+    with phase("mixer_0"):
+        for push_copy in plane_pushes:
+            push_copy.wait_recv()
+        for cols in (pl.ds(0, 512), pl.ds(512, 512)):
+            mixed_ref[:, cols] = jnp.dot(
+                pooled_rows[...],
+                w_plane[:, :, cols].reshape(1024, 512),
+                preferred_element_type=jnp.float32,
+            ).astype(jnp.bfloat16)
     for h in range(2):
         wait_for(w_mix.at[h, pl.ds(0, 448)], sib_mix.at[h, 0])
     with phase("mixer"):
@@ -470,10 +556,7 @@
     with phase("mixer_2"):
         for h in range(2):
             last = jnp.dot(pooled_rows[:, 896:], w_mix[h, 896:], preferred_element_type=jnp.float32)
-            mixed_ref[:, pl.ds(h * 1024, 1024)] = (mixed_sum[h] + last).astype(jnp.bfloat16)
-    with phase("combine_3"):
-        combine(3)
-
+            mixed_ref[:, pl.ds(1024 + h * 512, 512)] = (mixed_sum[h] + last).astype(jnp.bfloat16)
     for name in names:
         if name in "gu":
             sent, pushed = outgoing.at[pl.ds(0, 7 * 64)], outgoing.at[pl.ds(0, 8 * 64)]
@@ -484,9 +567,16 @@
         wait_for(pushed, push_send.at[number[name]])
     wait_for(outgoing.at[pl.ds(CAP, 15 * CAP)], disp_send)
     halo_copy.wait_send()
+    wait_for(z_bytes, plane_send.at[0])
+    for copy in (*x_copies, *y_copies, *plane_pushes):
+        copy.wait_send()
     wait_for(pooled_all.at[pl.ds(64, 960)], pool_sem.at[0])
-    for q in range(4):
+    for q in range(3):
         wait_for(rows_out.at[q, pl.ds(CAP, 15 * CAP)], ret_send.at[q])
+    with phase("combine_3"):
+        combine(3)
+    with phase("end"):
+        wait_for(rows_out.at[3, pl.ds(CAP, 15 * CAP)], ret_send.at[3])
 
 
 def body(
@@ -519,7 +609,8 @@
         scratch_shapes=[
             pltpu.VMEM((8, 256, width), bf),
             pltpu.VMEM((4, 1024, 512), bf),
-            pltpu.VMEM((2, 1024, 1024), bf),
+            pltpu.VMEM((2, 1024, 512), bf),
+            pltpu.VMEM((8, 128, 1024), bf),
             pltpu.VMEM((channels, rows_a), bf),
             pltpu.VMEM((channels, 128), bf),
             pltpu.VMEM((channels, rows_a), bf),
@@ -534,14 +625,16 @@
             pltpu.VMEM((4, slots, 512), bf),
             pltpu.VMEM((4, slots, 512), bf),
             pltpu.VMEM((rows_a // 16, 1024), bf),
-            pltpu.VMEM((2, rows_a // 16, 1024), f32),
-            dma((10,)),
+            pltpu.VMEM((2, rows_a // 16, 512), f32),
+            dma((11,)),
             dma((8, 8)),
             dma((8,)),
             dma((8,)),
             dma((2, 4)),
             dma((4,)),
             dma((2, 2)),
+            dma((11,)),
+            dma((11,)),
             dma,
             dma((2,)),
             dma((2,)),

time: 110 us -> 106 us (0.964)
  Pallas kernels: 107 us -> 104 us
    pallas_call x1, Pallas kernels: 107 us -> 104 us  [body(): pl.pallas_call(kernel, out_shape=(pltpu.VMEM((rows_a // 16, width), bf),...]
where the time goes in v3:
time: 106 us
  Pallas kernels  104 us (98%)
  local copies, waits for them, and re-layouts  1.77 us (2%)
    pallas_call x1, Pallas kernels, body(): pl.pallas_call(kernel, out_shape=(pltpu.VMEM((rows_a // 16, width), bf),...  104 us

profile of v3, /device:TPU:1, one launch (start us, length us, event | category | flops | bytes accessed | tf_op | source)
XLA Modules:
  0.0 106.1 jit_solution(13202566925067894443)
XLA Ops:
  0.6 103.7 %mixer_and_experts.1 = (bf16[128,2048]{1,0:T(8,128)(2,1)S(1)}, bf16[256,2048]{1,0:T(8,128)(2,1)S(1)}) custom-call(bf16[64,2048]{1,0:T(8,128)(2,1)} %bitcast.14, bf16[64,2048]{1,0:T(8,128)(2,1)} %bitcast.15, bf16[64,2048]{1,0:T(8,128)(2,1)} %bitcast.16, bf16[64,2048]{1,0:T(8,128)(2,1)} %mix_hbm.1, bf16[64,2048]{1,0:T(8,128)(2,1)} %bitcast.17, ...), custom_call_target="tpu_custom_call" | custom-call | tf_op jit(solution)/shard_map/mixer_and_experts/pallas_call | solution.py:601
  104.4 0.8 copy.14
  105.2 1.0 copy.15

commit v4 on v3

--- a/solution.py
+++ b/solution.py
@@ -31,11 +31,12 @@
 
 def kernel(
     gate_hbm, up_hbm, down_hbm, mix_hbm, pool_hbm, x_hbm,
-    pool_gain, moe_gain, ids_ref, route_ref,
+    pool_gain_hbm, moe_gain_hbm, ids_hbm, route_hbm,
     mixed_ref, moe_ref,
     w_in, w_down, w_mix, w_plane,
     pool_in, halo, pooled, pooled_all, x_in, normed, placing, picking,
     outgoing, arrived, hidden, rows_out, rows_back, pooled_rows, mixed_sum,
+    pool_gain, moe_gain, ids_ref, route_ref,
     load_sem, ring_recv, ring_send, push_send, sib_in, sib_down, sib_mix, plane_send, plane_recv,
     disp_send, disp_recv, halo_sem, pool_sem, ret_send, ret_recv,
 ):
@@ -93,6 +94,10 @@
     load("u", up_hbm, w_in.at[0, pl.ds(128, 64)])
     load("d0", down_hbm.at[:, pl.ds(0, 512)], w_down.at[0, pl.ds(0, 64)])
     load("x", x_hbm, x_in)
+    load("ids", ids_hbm, ids_ref)
+    load("moe_gain", moe_gain_hbm, moe_gain)
+    load("route", route_hbm, route_ref)
+    load("pool_gain", pool_gain_hbm, pool_gain)
     load("pool", pool_hbm, pool_in)
     for q in range(1, 4):
         load(f"d{q}", down_hbm.at[:, pl.ds(512 * q, 512)], w_down.at[q, pl.ds(0, 64)])
@@ -233,7 +238,8 @@
     for name in ("g", "u", "d0"):
         push(name, 0)
 
-    loads["x"].wait()
+    for name in ("x", "ids", "moe_gain", "route", "pool_gain"):
+        loads[name].wait()
     gain_row = moe_gain[...]
 
     def norm_rows(k, carry):
@@ -427,30 +433,31 @@
         copy.start()
     with phase("one_2b"):
         arrivals(2, *set_one[2:])
-    with phase("d1_1"):
-        arrivals(1, *both("d1"))
     with phase("disp_0"):
         wait_for(arrived.at[pl.ds(CAP, 7 * CAP)], disp_recv.at[0])
         in_ready(2)
     with phase("hid_a"):
         hidden_pairs(0, 0, 2)
-    with phase("one_3"):
-        arrivals(3, *set_one)
+    with phase("one_3a"):
+        arrivals(3, *set_one[:2])
     with phase("plane_x"):
         for copy in x_copies:
             copy.wait_recv()
     for copy in y_copies:
         copy.start()
+    with phase("one_3b"):
+        arrivals(3, *set_one[2:])
+    with phase("d1_1"):
+        arrivals(1, *both("d1"))
+    for q in (2, 3):
+        loads[f"d{q}"].wait()
+    first_sends(*both("d2"))
+    push("d2", 0)
+    push("d3", 0)
     with phase("in_3"):
         in_ready(3)
     with phase("hid_b"):
         hidden_pairs(0, 4, 1)
-    with phase("d1_2"):
-        arrivals(2, *both("d1"))
-    for q in (2, 3):
-        loads[f"d{q}"].wait()
-        first_sends(*both(f"d{q}"))
-        push(f"d{q}", 0)
     with phase("disp_1"):
         wait_for(arrived.at[pl.ds(8 * CAP, 8 * CAP)], disp_recv.at[1])
     with phase("hid_c"):
@@ -470,17 +477,23 @@
         down_ready(0)
     with phase("give_0a"):
         give_back(0, 0)
+    with phase("d1_2"):
+        arrivals(2, *both("d1"))
+    first_sends(*both("d3"))
     with phase("hid_67b"):
         hidden_pairs(1, 6, 1)
     with phase("give_0b"):
         give_back(0, 1)
-    with phase("two_1"):
+    with phase("d2_1"):
+        arrivals(1, *both("d2"))
+    with phase("d1_3"):
         arrivals(3, *both("d1"))
-        arrivals(1, *both("d2"))
+    with phase("d3_1"):
         arrivals(1, *both("d3"))
-    with phase("two_2"):
+    with phase("d2_2"):
+        arrivals(2, *both("d2"))
+    with phase("d1_4"):
         arrivals(4, *both("d1"))
-        arrivals(2, *both("d2"))
         down_ready(1)
     with phase("give_1a"):
         give_back(1, 0)
@@ -579,6 +592,21 @@
         wait_for(rows_out.at[3, pl.ds(CAP, 15 * CAP)], ret_send.at[3])
 
 
+def store_kernel(mixed_ref, moe_ref, mixed_hbm, moe_hbm, sems):
+    copies = []
+    for source, target, parts in ((moe_ref, moe_hbm, 4), (mixed_ref, mixed_hbm, 2)):
+        rows = source.shape[0] // parts
+        for k in range(parts):
+            part = pl.ds(k * rows, rows)
+            copies.append(
+                pltpu.make_async_copy(source.at[part], target.at[part], sems.at[len(copies)])
+            )
+    for copy in copies:
+        copy.start()
+    for copy in copies:
+        copy.wait()
+
+
 def body(
     pool_input,
     pool_gain,
@@ -598,13 +626,13 @@
     hbm = pl.BlockSpec(memory_space=pl.ANY)
     vmem = pl.BlockSpec(memory_space=pltpu.VMEM)
     dma = pltpu.SemaphoreType.DMA
-    return pl.pallas_call(
+    mixed, moe = pl.pallas_call(
         kernel,
         out_shape=(
             pltpu.VMEM((rows_a // 16, width), bf),
             pltpu.VMEM((tokens, width), bf),
         ),
-        in_specs=[hbm] * 6 + [vmem] * 4,
+        in_specs=[hbm] * 10,
         out_specs=(vmem, vmem),
         scratch_shapes=[
             pltpu.VMEM((8, 256, width), bf),
@@ -626,7 +654,11 @@
             pltpu.VMEM((4, slots, 512), bf),
             pltpu.VMEM((rows_a // 16, 1024), bf),
             pltpu.VMEM((2, rows_a // 16, 512), f32),
-            dma((11,)),
+            pltpu.VMEM((1, channels), f32),
+            pltpu.VMEM((1, width), f32),
+            pltpu.VMEM((2, tokens), jnp.int32),
+            pltpu.VMEM((2, tokens), f32),
+            dma((15,)),
             dma((8, 8)),
             dma((8,)),
             dma((8,)),
@@ -658,6 +690,17 @@
         expert_ids.T,
         route_weight.T,
     )
+    return pl.pallas_call(
+        store_kernel,
+        out_shape=(
+            jax.ShapeDtypeStruct(mixed.shape, bf),
+            jax.ShapeDtypeStruct(moe.shape, bf),
+        ),
+        in_specs=(vmem, vmem),
+        out_specs=(hbm, hbm),
+        scratch_shapes=[dma((6,))],
+        name="store",
+    )(*(pltpu.with_memory_space_constraint(a, pltpu.VMEM) for a in (mixed, moe)))
 
 
 def solution(mesh):

time: 106 us -> 104 us (0.981)
  local copies, waits for them, and re-layouts: 1.77 us -> 0 us
    unnamed x2 -> x0, local copies, waits for them, and re-layouts: 1.77 us -> none
    pallas_call x1, Pallas kernels: 104 us -> 102 us  [body(): pl.pallas_call(kernel, out_shape=(pltpu.VMEM((rows_a // 16, width), bf),...]
    pallas_call x0 -> x1, Pallas kernels: none -> 1.19 us  [body(): pl.pallas_call(store_kernel, out_shape=(jax.ShapeDtypeStruct(mixed.shape,...]
where the time goes in v4:
time: 104 us
  Pallas kernels  103 us (99%)
    pallas_call x1, Pallas kernels, body(): pl.pallas_call(kernel, out_shape=(pltpu.VMEM((rows_a // 16, width), bf),...  102 us

profile of v4, /device:TPU:1, one launch (start us, length us, event | category | flops | bytes accessed | tf_op | source)
XLA Modules:
  0.0 104.0 jit_solution(3492847403878368330)
XLA Ops:
  0.6 102.1 %mixer_and_experts.1 = (bf16[128,2048]{1,0:T(8,128)(2,1)S(1)}, bf16[256,2048]{1,0:T(8,128)(2,1)S(1)}) custom-call(bf16[64,2048]{1,0:T(8,128)(2,1)} %bitcast.14, bf16[64,2048]{1,0:T(8,128)(2,1)} %bitcast.15, bf16[64,2048]{1,0:T(8,128)(2,1)} %bitcast.16, bf16[64,2048]{1,0:T(8,128)(2,1)} %mix_hbm.1, bf16[64,2048]{1,0:T(8,128)(2,1)} %bitcast.17, ...), custom_call_target="tpu_custom_call" | custom-call | tf_op jit(solution)/shard_map/mixer_and_experts/pallas_call | solution.py:629
  102.8 1.2 %store.1 = (bf16[128,2048]{1,0:T(8,128)(2,1)}, bf16[256,2048]{1,0:T(8,128)(2,1)}) custom-call(bf16[128,2048]{1,0:T(8,128)(2,1)S(1)} %get-tuple-element.4.mixed_ref, bf16[256,2048]{1,0:T(8,128)(2,1)S(1)} %get-tuple-element.5.moe_ref), custom_call_target="tpu_custom_call" | custom-call | tf_op jit(solution)/shard_map/store/pallas_call | solution.py:693
